TPU v7x, 32 devices: a whole 2x2x4 slice. The times are simulated.
32 devices in a mesh: kv: 8 (over z, x), tp: 4 (over y, core).
Axes of the slice: x: 2, y: 2, z: 4, core: 2. Of those that a mesh axis runs over, the one named last changes fastest.
Arguments:
- tokens: bfloat16 [96, 4096], P(None, 'kv'), may hold values from -210 to 210
- norm_gain: float32 [4096], P('kv'), may hold values from 0.1 to 1.9
- w_query: bfloat16 [4096, 4096], P('kv', 'tp'), may hold values from -1 to 1
- w_key: bfloat16 [4096, 4096], P('kv', 'tp'), may hold values from -2 to 2
- w_value: bfloat16 [4096, 4096], P('kv', 'tp'), may hold values from -0.09375 to 0.09375
- w_output: bfloat16 [4096, 4096], P('tp', 'kv'), may hold values from -0.09375 to 0.09375
- cache_keys: bfloat16 [4, 4096, 4096], P(None, 'kv', 'tp'), may hold values from -820 to 820
- cache_values: bfloat16 [4, 4096, 4096], P(None, 'kv', 'tp'), may hold values from -6 to 6
- map_lambda: float32 [64], P('tp'), may hold values from 0.3 to 0.8
- out_gain: float32 [4096], P('tp'), may hold values from 0.1 to 1.9
- parents: int32 [4, 24], replicated, may hold values from -1 to 22, as said below
- lengths: int32 [4], replicated, may hold values from 2048 to 4048, as said below
- accepted: int32 [4], replicated, may hold values from 0 to 24
Outputs:
- mixed: bfloat16 [96, 4096], P(None, 'kv')
- new_keys: bfloat16 [4, 4096, 4096], P(None, 'kv', 'tp')
- new_values: bfloat16 [4, 4096, 4096], P(None, 'kv', 'tp')
Inputs may be any that keep to these rules, and one draw needn't show every extreme that they name: parents[b, j] lies between -1 and j - 1. `lengths`: some sequence has exactly the largest value.
All inputs are finite; a program needn't handle non-finite values.
Results may differ from a plain program's by a relative error of at most 0.029.
Values may be sent and summed in bfloat16 or wider, within the bound.
A program may use at most 128 MiB of HBM per device.

v0:
```python
import functools
import math

import jax
import jax.numpy as jnp
from jax import lax
from jax.experimental import pallas as pl
from jax.experimental.pallas import tpu as pltpu
from jax.sharding import PartitionSpec as P

HEAD = 64
QK = 32
LANES = 128
epsilon = 1e-05
masked_low = -1e30
MESH = pl.DeviceIdType.MESH
f32 = jnp.float32
bf16 = jnp.bfloat16


def iota(shape, dim):
    return lax.broadcasted_iota(jnp.int32, shape, dim)


def greet(axes):
    barrier = pltpu.get_barrier_semaphore()
    count = 0
    for axis, n in axes:
        me = lax.axis_index(axis)
        for k in range(1, n):
            pl.semaphore_signal(
                barrier, inc=1, device_id={axis: lax.rem(me + k, n)}, device_id_type=MESH
            )
            count += 1
    return barrier, count


def remote(src, dst, send_sem, recv_sem, axis, to):
    return pltpu.make_async_remote_copy(
        src_ref=src,
        dst_ref=dst,
        send_sem=send_sem,
        recv_sem=recv_sem,
        device_id={axis: to},
        device_id_type=MESH,
    )


def main_kernel(
    n, t, cols, seqs, prop, features,
    tok_ref, gain_ref, lam_ref, out_gain_ref, parent_ref, len_ref, acc_ref,
    wq_hbm, wk_hbm, wv_hbm, wo_hbm, keys_hbm, vals_hbm,
    out_ref, kv_ref,
    wbuf, wo_buf, kbuf, vbuf, q_part, q_recv, q_all, kv_part, kvx_recv, kv_sum, kvz_recv, sq_part, sq_recv,
    bv, bv_recv, st, st_part, st_recv, norm_all, out_part, out_recv,
    w_in, k_in, v_in, sq_s, sq_r, q_s, q_r, qa_s, qa_r, kx_s, kx_r, kz_s, kz_r, ax_s, ax_r, az_s, az_r,
    b_s, b_r, st_s, st_r, g_s, g_r, t_s, t_r,
):
    me = lax.axis_index("kv")
    mine = lax.axis_index("tp")
    groups = n // cols
    rows = tok_ref.shape[0]
    part = rows // groups
    per = seqs // groups
    both = 2 * prop
    _, length, width = kbuf.shape
    scale = QK ** (-0.5)
    peers = [lax.rem(me + k, n) for k in range(1, n)]
    inner_n = kv_ref.shape[0]
    outer_n = n // inner_n
    x, z = lax.rem(me, inner_n), me // inner_n
    x_peers = [lax.rem(x + k, inner_n) for k in range(1, inner_n)]
    z_peers = [lax.rem(z + k, outer_n) for k in range(1, outer_n)]
    barrier, count = greet((("kv", n), ("tp", t)))
    weights = [
        pltpu.make_async_copy(src, dst, w_in.at[i])
        for i, (src, dst) in enumerate(
            ((wq_hbm, wbuf.at[0]), (wk_hbm, wbuf.at[1]), (wv_hbm, wbuf.at[2]), (wo_hbm, wo_buf))
        )
    ]
    loads = []
    for b in range(seqs):
        loads.append(pltpu.make_async_copy(keys_hbm.at[b], kbuf.at[b], k_in.at[b]))
        loads.append(pltpu.make_async_copy(vals_hbm.at[b], vbuf.at[b], v_in.at[b]))
    for copy in weights + loads:
        copy.start()

    wide = tok_ref[...].astype(f32)
    square = jnp.sum(wide * wide, axis=1, keepdims=True)
    diagonal = iota((rows, LANES), 0) == iota((rows, LANES), 1)
    as_row = jnp.sum(jnp.where(diagonal, square, 0.0), axis=0, keepdims=True)
    sq_part[...] = jnp.broadcast_to(as_row, sq_part.shape)
    gained = (wide * gain_ref[...]).astype(bf16)

    def products(which, place):
        weights[which].wait()
        product = jnp.dot(gained, wbuf[which], preferred_element_type=f32)
        for c in range(cols):
            for r in range(groups):
                place(
                    c * groups + r,
                    product[r * part : (r + 1) * part, c * LANES : (c + 1) * LANES].astype(bf16),
                )

    def place_q(d, piece):
        q_part[d] = piece

    def place_k(d, piece):
        kv_part[d % inner_n, d // inner_n, :, :LANES] = piece

    def place_v(d, piece):
        kv_part[d % inner_n, d // inner_n, :, LANES:] = piece

    products(0, place_q)
    pl.semaphore_wait(barrier, count)
    sq_copies, q_copies = [], []
    for k, to in enumerate(peers):
        sq_copies.append(remote(sq_part, sq_recv.at[k], sq_s.at[k], sq_r.at[k], "kv", to))
        q_copies.append(remote(q_part.at[to], q_recv.at[k], q_s.at[k], q_r.at[k], "kv", to))
    for copy in sq_copies + q_copies:
        copy.start()
    products(1, place_k)
    products(2, place_v)
    kx_copies = [
        remote(kv_part.at[to], kvx_recv.at[k], kx_s.at[k], kx_r.at[k], "kv", z * inner_n + to)
        for k, to in enumerate(x_peers)
    ]
    for copy in kx_copies:
        copy.start()
    squares = sq_part[...]
    for k in range(n - 1):
        sq_copies[k].wait()
        squares = squares + sq_recv[k]
    first = lax.rem(me, groups) * part
    picked = iota((part, LANES), 0) + first == iota((part, LANES), 1)
    mean = jnp.sum(jnp.where(picked, squares[0:1], 0.0), axis=1, keepdims=True) / features
    factor = lax.rsqrt(mean + epsilon)
    total = q_part[me].astype(f32)
    for k in range(n - 1):
        q_copies[k].wait()
        total = total + q_recv[k].astype(f32)
    q_all[me] = (total * factor).astype(bf16)
    gathers = [
        remote(q_all.at[me], q_all.at[me], qa_s.at[k], qa_r.at[k], "kv", to)
        for k, to in enumerate(peers)
    ]
    for copy in gathers:
        copy.start()
    for copy in kx_copies:
        copy.wait()
    for i in range(outer_n):
        summed = kv_part[x, i].astype(f32)
        for k in range(inner_n - 1):
            summed = summed + kvx_recv[k, i].astype(f32)
        kv_sum[i] = summed.astype(bf16)
    kz_copies = [
        remote(kv_sum.at[to], kvz_recv.at[k], kz_s.at[k], kz_r.at[k], "kv", to * inner_n + x)
        for k, to in enumerate(z_peers)
    ]
    for copy in kz_copies:
        copy.start()

    lane = iota((1, LANES), 1)
    low = lane < HEAD
    own_first = lax.rem(me, groups) * per
    small_eye = iota((prop, prop), 0) == iota((prop, prop), 1)
    parent_rows = []
    for b in range(per):
        line = parent_ref[pl.ds(own_first + b, 1), :]
        parent_rows.append(
            jnp.sum(jnp.where(small_eye, line, 0), axis=1, keepdims=True)
        )
    parent = jnp.concatenate(parent_rows, axis=0)
    shape = (part, part)
    target = jnp.concatenate([p + b * prop for b, p in enumerate(parent_rows)], axis=0)
    link = (parent >= 0) & (target == iota(shape, 1))
    reach = jnp.where(link | (iota(shape, 0) == iota(shape, 1)), 1.0, 0.0)
    power = 1
    while power < prop:
        reach = jnp.minimum(
            jnp.dot(reach.astype(bf16), reach.astype(bf16), preferred_element_type=f32), 1.0
        )
        power *= 2
    lineage = jnp.concatenate([reach] * 4, axis=0) > 0.5
    st[...] = jnp.zeros_like(st)

    for copy in gathers:
        copy.wait()
    wide_lane = iota((1, 2 * LANES), 1)
    b_copies = []
    pieces = seqs if groups == 1 else 1
    tall = per * both // pieces

    def send_piece(piece):
        for k, to in enumerate(peers):
            c, r = to // groups, lax.rem(to, groups)
            span = pl.ds(piece * tall, tall)
            copy = remote(
                bv.at[c, r, span], bv_recv.at[k, span], b_s.at[k, piece], b_r.at[k, piece], "kv", to
            )
            copy.start()
            b_copies.append(copy)

    for b in range(seqs):
        r, inner = b // per, b % per
        begin = inner * prop
        rel = len_ref[b] + acc_ref[b] - me * length
        visible = iota((1, length), 1) < rel
        loads[2 * b].wait()
        loads[2 * b + 1].wait()
        for g in range(width // (2 * LANES)):
            span = slice(g * 2 * LANES, (g + 1) * 2 * LANES)
            query = jnp.concatenate(
                [
                    q_all[c * groups + r].astype(f32)[begin : begin + prop]
                    for c in (2 * g, 2 * g + 1)
                ],
                axis=1,
            )
            spread = jnp.concatenate(
                [jnp.where(wide_lane // QK == i, query, 0.0) for i in range(2 * LANES // QK)],
                axis=0,
            ).astype(bf16)
            scores = lax.dot_general(
                spread, kbuf[b, :, span], (((1,), (1,)), ((), ())), preferred_element_type=f32
            )
            scores = jnp.where(visible, scores * scale, masked_low)
            largest = jnp.max(scores, axis=1, keepdims=True)
            weight = jnp.where(visible, jnp.exp(scores - largest), 0.0)
            total = jnp.sum(weight, axis=1, keepdims=True)
            summed = jnp.dot(weight.astype(bf16), vbuf[b, :, span], preferred_element_type=f32)
            merged = jnp.zeros((both, 2 * LANES), f32)
            for h in range(2 * LANES // HEAD):
                piece = slice(h * both, (h + 1) * both)
                merged = jnp.where(wide_lane // HEAD == h, summed[piece], merged)
                c = g * 2 + h // 2
                at = inner * 4 + h % 2
                stat = st[c, r, :both]
                stat = jnp.where(lane == at, largest[piece], stat)
                st[c, r, :both] = jnp.where(lane == at + 2, total[piece], stat)
            merged = merged.astype(bf16)
            for half in range(2):
                bv[g * 2 + half, r, inner * both : (inner + 1) * both, :] = merged[
                    :, half * LANES : (half + 1) * LANES
                ]
        if groups == 1 and b < seqs - 1:
            send_piece(b)
    kept = 4 * per
    kept = -(-kept // 8) * 8
    for c in range(cols):
        for r in range(groups):
            st_part[c, r] = jnp.transpose(st[c, r])[:kept]
    st_copies = []
    for k, to in enumerate(peers):
        c, r = to // groups, lax.rem(to, groups)
        st_copies.append(remote(st_part.at[c, r], st_recv.at[k], st_s.at[k], st_r.at[k], "kv", to))
        st_copies[k].start()
    send_piece(pieces - 1)

    own = kv_sum[z].astype(f32)
    for k in range(outer_n - 1):
        kz_copies[k].wait()
        own = own + kvz_recv[k].astype(f32)
    own = (own * factor).astype(bf16)
    kv_ref[x, z] = own
    az_copies = [
        remote(kv_ref.at[x, z], kv_ref.at[x, z], az_s.at[k], az_r.at[k], "kv", to * inner_n + x)
        for k, to in enumerate(z_peers)
    ]
    for copy in az_copies:
        copy.start()
    query = q_all[me].astype(f32)
    spread = jnp.concatenate(
        [jnp.where(lane // QK == i, query, 0.0) for i in range(4)], axis=0
    ).astype(bf16)
    scores = lax.dot_general(
        spread, own[:, :LANES], (((1,), (1,)), ((), ())), preferred_element_type=f32
    )
    scores = jnp.where(lineage, scores * scale, masked_low)
    top = jnp.max(scores, axis=1, keepdims=True)
    weight = jnp.where(lineage, jnp.exp(scores - top), 0.0)
    total = jnp.sum(weight, axis=1, keepdims=True)
    summed = jnp.dot(weight.astype(bf16), own[:, LANES:], preferred_element_type=f32)

    def laid(array):
        found = []
        for b in range(per):
            for m in range(2):
                s0 = slice(m * part + b * prop, m * part + (b + 1) * prop)
                s1 = slice((2 + m) * part + b * prop, (2 + m) * part + (b + 1) * prop)
                found.append(jnp.where(low, array[s0], array[s1]))
        return jnp.concatenate(found, axis=0)

    tops, totals, sums = [laid(top)], [laid(total)], [laid(summed)]

    def take(stats, values):
        for which, into in ((0, tops), (2, totals)):
            into.append(
                jnp.concatenate(
                    [
                        jnp.where(
                            low,
                            stats[:both, b * 4 + which : b * 4 + which + 1],
                            stats[:both, b * 4 + which + 1 : b * 4 + which + 2],
                        )
                        for b in range(per)
                    ],
                    axis=0,
                )
            )
        sums.append(values.astype(f32))

    col, row = me // groups, lax.rem(me, groups)
    take(st[col, row], bv[col, row])
    filler = jnp.zeros((LANES - kept, LANES), f32)
    for copy in st_copies + b_copies:
        copy.wait()
    for k in range(n - 1):
        take(jnp.transpose(jnp.concatenate([st_recv[k], filler], axis=0)), bv_recv[k])
    highest = functools.reduce(jnp.maximum, tops)
    denominator = jnp.zeros_like(highest)
    numerator = jnp.zeros_like(highest)
    for a, b, c in zip(tops, totals, sums):
        share = jnp.exp(a - highest)
        denominator = denominator + b * share
        numerator = numerator + c * share
    attended = numerator / denominator
    heads = iota(lam_ref.shape, 1)
    lam_low = jnp.sum(jnp.where(heads == 2 * col, lam_ref[...], 0.0), axis=1, keepdims=True)
    lam_high = jnp.sum(jnp.where(heads == 2 * col + 1, lam_ref[...], 0.0), axis=1, keepdims=True)
    lam = jnp.where(low, lam_low, lam_high)
    gain = out_gain_ref[:, pl.ds(pl.multiple_of(col * LANES, LANES), LANES)]
    difference = jnp.concatenate(
        [
            attended[b * both : b * both + prop] - lam * attended[b * both + prop : (b + 1) * both]
            for b in range(per)
        ],
        axis=0,
    )
    squared = difference * difference
    one = jnp.sum(jnp.where(low, squared, 0.0), axis=1, keepdims=True)
    two = jnp.sum(jnp.where(low, 0.0, squared), axis=1, keepdims=True)
    mean = jnp.where(low, one, two) / HEAD
    norm_all[me] = (difference * lax.rsqrt(mean + epsilon) * gain).astype(bf16)
    gathers = [
        remote(norm_all.at[me], norm_all.at[me], g_s.at[k], g_r.at[k], "kv", to)
        for k, to in enumerate(peers)
    ]
    for copy in gathers:
        copy.start()
    late = [
        remote(kv_ref.at[x], kv_ref.at[x], ax_s.at[k], ax_r.at[k], "kv", z * inner_n + to)
        for k, to in enumerate(x_peers)
    ]
    for copy in az_copies:
        copy.wait()
    for copy in late:
        copy.start()
    weights[3].wait()
    for copy in gathers:
        copy.wait()
    normed = jnp.concatenate(
        [
            jnp.concatenate([norm_all[c * groups + r] for r in range(groups)], axis=0)
            for c in range(cols)
        ],
        axis=1,
    )
    out_part[...] = jnp.dot(normed, wo_buf[...], preferred_element_type=f32).astype(bf16)
    copies = []
    for k in range(1, t):
        to = lax.rem(mine + k, t)
        copies.append(remote(out_part, out_recv.at[k], t_s.at[k], t_r.at[k], "tp", to))
    for copy in copies:
        copy.start()
    mixed = out_part[...].astype(f32)
    for k in range(1, t):
        copies[k - 1].wait()
        mixed = mixed + out_recv[k].astype(f32)
    out_ref[...] = mixed.astype(bf16)
    for copy in late:
        copy.wait()


def place_kernel(
    groups, prop, len_ref, acc_ref, kv_ref, keys_hbm, vals_hbm, nk_hbm, nv_hbm,
    kbuf, vbuf, k_in, v_in, k_out, v_out,
):
    seqs, length, width = kbuf.shape
    cols = width // LANES
    per = seqs // groups
    inner_n = kv_ref.shape[0]
    offset = lax.axis_index("kv") * length
    loads = []
    for b in range(seqs):
        loads.append(pltpu.make_async_copy(keys_hbm.at[b], kbuf.at[b], k_in.at[b]))
        loads.append(pltpu.make_async_copy(vals_hbm.at[b], vbuf.at[b], v_in.at[b]))
    for copy in loads:
        copy.start()
    stores = []
    window = 48
    for b in range(seqs):
        r, begin = b // per, (b % per) * prop
        rel = len_ref[b] + acc_ref[b] - offset
        base = jnp.clip((rel // 16) * 16, 0, length - window)
        at = pl.ds(pl.multiple_of(base, 16), window)
        slot = iota((window, prop), 0) + base - rel
        placing = (slot == iota((window, prop), 1)).astype(bf16)
        slot_col = iota((window, 1), 0) + base - rel
        inside = (slot_col >= 0) & (slot_col < prop)
        for which, buf in enumerate((kbuf, vbuf)):
            fresh = jnp.concatenate(
                [
                    kv_ref[
                        (c * groups + r) % inner_n,
                        (c * groups + r) // inner_n,
                        begin : begin + prop,
                        which * LANES : (which + 1) * LANES,
                    ]
                    for c in range(cols)
                ],
                axis=1,
            )
            moved = jnp.dot(placing, fresh, preferred_element_type=f32)
            loads[2 * b + which].wait()
            old = buf[b, at, :].astype(f32)
            buf[b, at, :] = jnp.where(inside, moved, old).astype(bf16)
            into, sem = ((nk_hbm, k_out), (nv_hbm, v_out))[which]
            stores.append(pltpu.make_async_copy(buf.at[b], into.at[b], sem.at[b]))
            stores[-1].start()
    for copy in stores:
        copy.wait()


def local(
    n, t, tokens, norm_gain, w_query, w_key, w_value, w_output, cache_keys, cache_values,
    map_lambda, out_gain, parents, lengths, accepted,
):
    rows, depth = tokens.shape
    seqs, length, width = cache_keys.shape
    prop = rows // seqs
    both = 2 * prop
    cols = min(n, width // LANES)
    groups = n // cols
    part = rows // groups
    per = seqs // groups
    pieces = seqs if groups == 1 else 1
    kept = -(-4 * per // 8) * 8
    out_cols = w_output.shape[1]
    inner_n = math.gcd(n, 1 << (n.bit_length() - 1) // 2)
    outer_n = n // inner_n
    vmem = pl.BlockSpec(memory_space=pltpu.VMEM)
    smem = pl.BlockSpec(memory_space=pltpu.SMEM)
    hbm = pl.BlockSpec(memory_space=pl.ANY)
    dma = pltpu.SemaphoreType.DMA
    V = pltpu.VMEM
    mixed, gathered = pl.pallas_call(
        functools.partial(main_kernel, n, t, cols, seqs, prop, depth * n),
        name="attend",
        out_shape=(
            jax.ShapeDtypeStruct((rows, out_cols), bf16),
            jax.ShapeDtypeStruct((inner_n, outer_n, part, 2 * LANES), bf16),
        ),
        in_specs=[vmem] * 5 + [smem] * 2 + [hbm] * 6,
        out_specs=(vmem, vmem),
        scratch_shapes=[
            V((3, depth, width), bf16),
            V(w_output.shape, bf16),
            V(cache_keys.shape, bf16),
            V(cache_values.shape, bf16),
            V((n, part, LANES), bf16),
            V((n, part, LANES), bf16),
            V((n, part, LANES), bf16),
            V((inner_n, outer_n, part, 2 * LANES), bf16),
            V((inner_n, outer_n, part, 2 * LANES), bf16),
            V((outer_n, part, 2 * LANES), bf16),
            V((outer_n, part, 2 * LANES), bf16),
            V((8, LANES), f32),
            V((n, 8, LANES), f32),
            V((cols, groups, per * both, LANES), bf16),
            V((n, per * both, LANES), bf16),
            V((cols, groups, LANES, LANES), f32),
            V((cols, groups, kept, LANES), f32),
            V((n, kept, LANES), f32),
            V((n, part, LANES), bf16),
            V((rows, out_cols), bf16),
            V((t, rows, out_cols), bf16),
            dma((4,)),
            dma((seqs,)),
            dma((seqs,)),
        ]
        + [dma((n,))] * 14
        + [dma((n, pieces))] * 2
        + [dma((n,))] * 4
        + [dma((t,))] * 2,
        compiler_params=pltpu.CompilerParams(collective_id=0, has_side_effects=True),
    )(
        tokens, norm_gain[None], map_lambda[None], out_gain[None], parents, lengths, accepted,
        w_query, w_key, w_value, w_output, cache_keys, cache_values,
    )
    new_keys, new_values = pl.pallas_call(
        functools.partial(place_kernel, groups, prop),
        name="place",
        out_shape=(
            jax.ShapeDtypeStruct(cache_keys.shape, bf16),
            jax.ShapeDtypeStruct(cache_values.shape, bf16),
        ),
        in_specs=[smem, smem, vmem, hbm, hbm],
        out_specs=(hbm, hbm),
        scratch_shapes=[V(cache_keys.shape, bf16), V(cache_values.shape, bf16)]
        + [dma((seqs,))] * 4,
    )(lengths, accepted, gathered, cache_keys, cache_values)
    return (mixed, new_keys, new_values)


def solution(mesh):
    placed = (
        P(None, "kv"),
        P("kv"),
        P("kv", "tp"),
        P("kv", "tp"),
        P("kv", "tp"),
        P("tp", "kv"),
        P(None, "kv", "tp"),
        P(None, "kv", "tp"),
        P("tp"),
        P("tp"),
        P(),
        P(),
        P(),
    )
    return jax.shard_map(
        functools.partial(local, mesh.shape["kv"], mesh.shape["tp"]),
        mesh=mesh,
        in_specs=placed,
        out_specs=(P(None, "kv"), P(None, "kv", "tp"), P(None, "kv", "tp")),
        check_vma=False,
    )
```

profile of v0, /device:TPU:0, one launch (start us, length us, event | category | flops | bytes accessed | tf_op | source)
XLA Modules:
  0.0 57.2 jit_solution(6195288257042874457)
XLA Ops:
  0.6 48.3 %attend.1 = (bf16[96,512]{1,0:T(8,128)(2,1)}, bf16[2,4,96,256]{3,2,1,0:T(8,128)(2,1)}) custom-call(bf16[96,512]{1,0:T(8,128)(2,1)} %tok_ref.1, f32[1,512]{1,0:T(1,128)} %bitcast.4, f32[1,16]{1,0:T(1,128)} %bitcast.5, f32[1,1024]{1,0:T(1,128)} %bitcast.3, s32[4,24]{1,0:T(4,128)} %parent_ref.1, s32[4]{0:T(128)} %len_ref.3, s32[4]{0:T(128)} %acc_ref.3, ...), custom_call_target="tpu_custom_call" | custom-call | tf_op jit(solution)/shard_map/attend/pallas_call | solution.py:457
  49.0 0.0 copy-start
  49.0 7.5 %place.1 = (bf16[4,512,1024]{2,1,0:T(8,128)(2,1)}, bf16[4,512,1024]{2,1,0:T(8,128)(2,1)}) custom-call(s32[4]{0:T(128)} %len_ref.3, s32[4]{0:T(128)} %acc_ref.3, bf16[2,4,96,256]{3,2,1,0:T(8,128)(2,1)} %get-tuple-element.8.kv_ref, bf16[4,512,1024]{2,1,0:T(8,128)(2,1)} %keys_hbm.3, bf16[4,512,1024]{2,1,0:T(8,128)(2,1)} %vals_hbm.3), custom_call_target="tpu_custom_call" | custom-call | tf_op jit(solution)/shard_map/place/pallas_call | solution.py:501
  56.5 0.0 copy-done
  56.5 0.6 %copy.17 = bf16[96,512]{1,0:T(8,128)(2,1)} copy(bf16[96,512]{1,0:T(8,128)(2,1)S(1)} %copy-done) | data formatting | bytes 196608
Async XLA Ops:
  49.0 7.6 %copy-start = (bf16[96,512]{1,0:T(8,128)(2,1)S(1)}, bf16[96,512]{1,0:T(8,128)(2,1)}, u32[]{:S(2)}) copy-start(bf16[96,512]{1,0:T(8,128)(2,1)} %get-tuple-element.14) | copy-start | bytes 294916
where the time goes:
time: 57.7 us; the launch traced here: 57.2 us
  Pallas kernels  55.9 us (97%)
  between operations  0.67 us (1%)
  local copies, waits for them, and re-layouts  0.65 us (1%)
    pallas_call x1, Pallas kernels, local(): pl.pallas_call(functools.partial(main_kernel, n, t, cols, seqs, prop, dep...  48.3 us
    pallas_call x1, Pallas kernels, local(): pl.pallas_call(functools.partial(place_kernel, groups, prop), name='place...  7.53 us

commit v1 on v0

v1 whole, which is shorter than its diff:
```python
import functools
import math

import jax
import jax.numpy as jnp
from jax import lax
from jax.experimental import pallas as pl
from jax.experimental.pallas import tpu as pltpu
from jax.sharding import PartitionSpec as P

HEAD = 64
QK = 32
LANES = 128
epsilon = 1e-05
masked_low = -1e30
MESH = pl.DeviceIdType.MESH
f32 = jnp.float32
bf16 = jnp.bfloat16


def iota(shape, dim):
    return lax.broadcasted_iota(jnp.int32, shape, dim)


def greet(axes):
    barrier = pltpu.get_barrier_semaphore()
    count = 0
    for axis, n in axes:
        me = lax.axis_index(axis)
        for k in range(1, n):
            pl.semaphore_signal(
                barrier, inc=1, device_id={axis: lax.rem(me + k, n)}, device_id_type=MESH
            )
            count += 1
    return barrier, count


def remote(src, dst, send_sem, recv_sem, axis, to):
    return pltpu.make_async_remote_copy(
        src_ref=src,
        dst_ref=dst,
        send_sem=send_sem,
        recv_sem=recv_sem,
        device_id={axis: to},
        device_id_type=MESH,
    )


def drain(ref, sem):
    pltpu.make_async_copy(ref, ref, sem).wait()


def flip(i, bit):
    return i + bit - 2 * bit * lax.rem(i // bit, 2)


def main_kernel(
    n, t, cols, seqs, prop, features, inner_n,
    tok_hbm, gain_hbm, lam_hbm, out_gain_hbm, parent_hbm, len_hbm, acc_hbm,
    wq_hbm, wk_hbm, wv_hbm, wo_hbm, keys_hbm, vals_hbm,
    out_ref, kv_ref, kbuf, vbuf, len_out, acc_out,
    tok_ref, gain_ref, lam_ref, out_gain_ref, parent_ref, len_ref, acc_ref,
    wbuf, wo_buf, q_part, q_recv, q_all, kv_part, kvx_recv, kv_sum, kvz_recv, sq_all,
    bv, bv_recv, st, st_recv, self_v, self_st, norm_all, out_part, out_recv,
    s_in, w_in, k_in, v_in, sq_s, sq_r, q_s, q_r, qa_s, qa_r, kx_s, kx_r, kz_s, kz_r, up_s, up_r, ag_s, ag_r,
    b_s, b_r, st_s, st_r, g_s, g_r, t_s, t_r,
):
    me = lax.axis_index("kv")
    mine = lax.axis_index("tp")
    groups = n // cols
    rows = tok_ref.shape[0]
    part = rows // groups
    per = seqs // groups
    both = 2 * prop
    _, length, width = kbuf.shape
    scale = QK ** (-0.5)
    peers = [lax.rem(me + k, n) for k in range(1, n)]
    outer_n = n // inner_n
    half = outer_n // 2
    x, z = lax.rem(me, inner_n), me // inner_n
    x_peers = [lax.rem(x + k, inner_n) for k in range(1, inner_n)]
    slot = lax.rem(z, half) * inner_n + x
    flat = half * inner_n - 1
    barrier, count = greet((("kv", n), ("tp", t)))
    weights = [
        pltpu.make_async_copy(src, dst, w_in.at[i])
        for i, (src, dst) in enumerate(
            ((wq_hbm, wbuf.at[0]), (wk_hbm, wbuf.at[1]), (wv_hbm, wbuf.at[2]), (wo_hbm, wo_buf))
        )
    ]
    small = [
        pltpu.make_async_copy(src, dst, s_in.at[i])
        for i, (src, dst) in enumerate(
            (
                (tok_hbm, tok_ref), (gain_hbm, gain_ref), (lam_hbm, lam_ref), (out_gain_hbm, out_gain_ref),
                (parent_hbm, parent_ref), (len_hbm, len_ref), (acc_hbm, acc_ref), (len_hbm, len_out), (acc_hbm, acc_out),
            )
        )
    ]
    order = [r * per + p for p in range(per) for r in range(groups)]
    loads = {}
    for b in order:
        loads[b] = (
            pltpu.make_async_copy(keys_hbm.at[b], kbuf.at[b], k_in.at[b]),
            pltpu.make_async_copy(vals_hbm.at[b], vbuf.at[b], v_in.at[b]),
        )
    for copy in small[:2] + weights[:1] + small[2:] + weights[1:3]:
        copy.start()
    for b in order:
        for copy in loads[b]:
            copy.start()
    weights[3].start()
    for copy in small[:2]:
        copy.wait()

    wide = tok_ref[...].astype(f32)
    square = jnp.sum(wide * wide, axis=1, keepdims=True)
    diagonal = iota((rows, LANES), 0) == iota((rows, LANES), 1)
    as_row = jnp.sum(jnp.where(diagonal, square, 0.0), axis=0, keepdims=True)
    sq_all[me] = as_row
    gained = (wide * gain_ref[...]).astype(bf16)

    def products(which, place):
        weights[which].wait()
        product = jnp.dot(gained, wbuf[which], preferred_element_type=f32)
        for c in range(cols):
            for b in range(seqs):
                place(
                    b % per,
                    c * groups + b // per,
                    product[b * prop : (b + 1) * prop, c * LANES : (c + 1) * LANES].astype(bf16),
                )

    def place_q(p, d, piece):
        q_part[p, d] = piece

    def place_k(p, d, piece):
        kv_part[d % inner_n, d // inner_n, p * prop : (p + 1) * prop, :LANES] = piece

    def place_v(p, d, piece):
        kv_part[d % inner_n, d // inner_n, p * prop : (p + 1) * prop, LANES:] = piece

    products(0, place_q)
    pl.semaphore_wait(barrier, count)
    for to in peers:
        remote(sq_all.at[me], sq_all.at[me], sq_s, sq_r, "kv", to).start()
    for p in range(per):
        for k, to in enumerate(peers):
            remote(q_part.at[p, to], q_recv.at[p, k], q_s, q_r.at[p], "kv", to).start()
    products(1, place_k)
    products(2, place_v)
    for k, to in enumerate(x_peers):
        remote(kv_part.at[to], kvx_recv.at[k], kx_s, kx_r, "kv", z * inner_n + to).start()

    lane = iota((1, LANES), 1)
    low = lane < HEAD
    for copy in small[2:]:
        copy.wait()
    own_first = lax.rem(me, groups) * per
    small_eye = iota((prop, prop), 0) == iota((prop, prop), 1)
    parent_rows = []
    for b in range(per):
        line = parent_ref[pl.ds(own_first + b, 1), :]
        parent_rows.append(
            jnp.sum(jnp.where(small_eye, line, 0), axis=1, keepdims=True)
        )
    parent = jnp.concatenate(parent_rows, axis=0)
    shape = (part, part)
    target = jnp.concatenate([p + b * prop for b, p in enumerate(parent_rows)], axis=0)
    link = (parent >= 0) & (target == iota(shape, 1))
    reach = jnp.where(link | (iota(shape, 0) == iota(shape, 1)), 1.0, 0.0)
    power = 1
    while power < prop:
        reach = jnp.minimum(
            jnp.dot(reach.astype(bf16), reach.astype(bf16), preferred_element_type=f32), 1.0
        )
        power *= 2
    lineage = jnp.concatenate([reach] * 4, axis=0) > 0.5

    drain(sq_all.at[pl.ds(0, n - 1)], sq_r)
    squares = sq_all[0]
    for k in range(1, n):
        squares = squares + sq_all[k]
    first = lax.rem(me, groups) * part
    picked = iota((part, LANES), 0) + first == iota((part, LANES), 1)
    mean = jnp.sum(jnp.where(picked, squares, 0.0), axis=1, keepdims=True) / features
    factor = lax.rsqrt(mean + epsilon)
    for p in range(per):
        drain(q_recv.at[p], q_r.at[p])
        total = q_part[p, me].astype(f32)
        for k in range(n - 1):
            total = total + q_recv[p, k].astype(f32)
        q_all[p, me] = (total * factor[p * prop : (p + 1) * prop]).astype(bf16)
        for to in peers:
            remote(q_all.at[p, me], q_all.at[p, me], qa_s, qa_r.at[p], "kv", to).start()

    def kv_across_x():
        drain(kvx_recv, kx_r)
        for i in range(outer_n):
            summed = kv_part[x, i].astype(f32)
            for k in range(inner_n - 1):
                summed = summed + kvx_recv[k, i].astype(f32)
            kv_sum[i] = summed.astype(bf16)

    chunks = [z]
    bits = []
    bit = 1
    while bit < outer_n:
        bits.append(bit)
        bit *= 2
    live = {}
    for s in reversed(range(len(bits))):
        live[s] = list(chunks)
        chunks = chunks + [flip(c, bits[s]) for c in chunks]

    def kv_send(s):
        partner = flip(z, bits[s])
        for i, c in enumerate(live[s]):
            remote(
                kv_sum.at[flip(c, bits[s])], kvz_recv.at[s, i], kz_s.at[s], kz_r.at[s], "kv", partner * inner_n + x
            ).start()

    def kv_take(s):
        size = len(live[s])
        drain(kvz_recv.at[s, pl.ds(0, size)], kz_r.at[s])
        drain(kvz_recv.at[s, pl.ds(0, size)], kz_s.at[s])
        for i, c in enumerate(live[s]):
            kv_sum[c] = (kv_sum[c].astype(f32) + kvz_recv[s, i].astype(f32)).astype(bf16)

    wide_lane = iota((1, 2 * LANES), 1)

    def attend(p):
        stat = jnp.zeros((both, LANES), f32)
        for r in range(groups):
            b = r * per + p
            rel = len_ref[b] + acc_ref[b] - me * length
            visible = iota((1, length), 1) < rel
            for copy in loads[b]:
                copy.wait()
            for g in range(width // (2 * LANES)):
                span = slice(g * 2 * LANES, (g + 1) * 2 * LANES)
                query = jnp.concatenate(
                    [q_all[p, c * groups + r].astype(f32) for c in (2 * g, 2 * g + 1)], axis=1
                )
                spread = jnp.concatenate(
                    [jnp.where(wide_lane // QK == i, query, 0.0) for i in range(2 * LANES // QK)],
                    axis=0,
                ).astype(bf16)
                scores = lax.dot_general(
                    spread, kbuf[b, :, span], (((1,), (1,)), ((), ())), preferred_element_type=f32
                )
                scores = jnp.where(visible, scores * scale, masked_low)
                largest = jnp.max(scores, axis=1, keepdims=True)
                weight = jnp.where(visible, jnp.exp(scores - largest), 0.0)
                total = jnp.sum(weight, axis=1, keepdims=True)
                summed = jnp.dot(weight.astype(bf16), vbuf[b, :, span], preferred_element_type=f32)
                merged = jnp.zeros((both, 2 * LANES), f32)
                for h in range(2 * LANES // HEAD):
                    piece = slice(h * both, (h + 1) * both)
                    merged = jnp.where(wide_lane // HEAD == h, summed[piece], merged)
                    at = ((2 * g + h // 2) * groups + r) * 4 + h % 2
                    stat = jnp.where(lane == at, largest[piece], stat)
                    stat = jnp.where(lane == at + 2, total[piece], stat)
                merged = merged.astype(bf16)
                for c in range(2):
                    bv[p, (2 * g + c) * groups + r] = merged[:, c * LANES : (c + 1) * LANES]
        turned = jnp.transpose(
            jnp.concatenate([stat, jnp.zeros((LANES - both, LANES), f32)], axis=0)
        )
        for d in range(n):
            st[p, d] = turned[4 * d : 4 * d + 4]
        for k, to in enumerate(peers):
            remote(st.at[p, to], st_recv.at[p, k], st_s, st_r.at[p], "kv", to).start()
        for k, to in enumerate(peers):
            remote(bv.at[p, to], bv_recv.at[p, k], b_s, b_r.at[p], "kv", to).start()

    def tree():
        own = (kv_sum[z].astype(f32) * factor).astype(bf16)
        kv_ref[slot, z // half] = own
        query = jnp.concatenate([q_all[p, me] for p in range(per)], axis=0).astype(f32)
        spread = jnp.concatenate(
            [jnp.where(lane // QK == i, query, 0.0) for i in range(4)], axis=0
        ).astype(bf16)
        scores = lax.dot_general(
            spread, own[:, :LANES], (((1,), (1,)), ((), ())), preferred_element_type=f32
        )
        scores = jnp.where(lineage, scores * scale, masked_low)
        top = jnp.max(scores, axis=1, keepdims=True)
        weight = jnp.where(lineage, jnp.exp(scores - top), 0.0)
        total = jnp.sum(weight, axis=1, keepdims=True)
        summed = jnp.dot(weight.astype(bf16), own[:, LANES:], preferred_element_type=f32)
        stat = jnp.zeros((both, LANES), f32)
        for p in range(per):
            cut = [slice(i * part + p * prop, i * part + (p + 1) * prop) for i in range(4)]

            def laid(array, head):
                return jnp.concatenate([array[cut[2 * head]], array[cut[2 * head + 1]]], axis=0)

            self_v[p] = jnp.where(low, laid(summed, 0), laid(summed, 1))
            for h in range(2):
                stat = jnp.where(lane == 4 * p + h, laid(top, h), stat)
                stat = jnp.where(lane == 4 * p + 2 + h, laid(total, h), stat)
        turned = jnp.transpose(
            jnp.concatenate([stat, jnp.zeros((LANES - both, LANES), f32)], axis=0)
        )
        for p in range(per):
            self_st[p] = turned[4 * p : 4 * p + 4]

    def kv_up():
        @pl.when(z < half)
        def _():
            remote(kv_ref.at[slot, 0], kv_ref.at[slot, 0], up_s, up_r, "kv", me + half * inner_n).start()

    def kv_spread():

        @pl.when(z >= half)
        def _():
            drain(kv_ref.at[slot, 0], up_r)
            for k in range(1, flat + 1):
                to = half * inner_n + lax.rem(slot + k, flat + 1)
                remote(kv_ref.at[slot], kv_ref.at[slot], ag_s, ag_r, "kv", to).start()

    def kv_end():

        @pl.when(z < half)
        def _():
            drain(kv_ref.at[slot, 0], up_s)

        @pl.when(z >= half)
        def _():
            for sem in (ag_r, ag_s):
                drain(kv_ref.at[pl.ds(0, flat)], sem)

    col = me // groups
    heads = iota(lam_ref.shape, 1)
    lam_low = jnp.sum(jnp.where(heads == 2 * col, lam_ref[...], 0.0), axis=1, keepdims=True)
    lam_high = jnp.sum(jnp.where(heads == 2 * col + 1, lam_ref[...], 0.0), axis=1, keepdims=True)
    lam = jnp.where(low, lam_low, lam_high)
    gain = out_gain_ref[:, pl.ds(pl.multiple_of(col * LANES, LANES), LANES)]

    def merge(p):
        drain(st_recv.at[p], st_r.at[p])
        drain(bv_recv.at[p], b_r.at[p])
        stats = [st[p, me]] + [st_recv[p, k] for k in range(n - 1)] + [self_st[p]]
        highest = functools.reduce(jnp.maximum, [a[:2] for a in stats])
        shares = [jnp.exp(a[:2] - highest) for a in stats]
        denominator = functools.reduce(lambda a, b: a + b, [a * b[2:] for a, b in zip(shares, stats)])
        inverse = 1.0 / denominator
        shares = [a * inverse for a in shares]
        filler = jnp.zeros((LANES - 2 * len(shares), LANES), f32)
        turned = jnp.transpose(jnp.concatenate(shares + [filler], axis=0))
        values = [bv[p, me]] + [bv_recv[p, k] for k in range(n - 1)] + [self_v[p]]
        attended = jnp.zeros((both, LANES), f32)
        for i, value in enumerate(values):
            share = jnp.where(low, turned[:both, 2 * i : 2 * i + 1], turned[:both, 2 * i + 1 : 2 * i + 2])
            attended = attended + value.astype(f32) * share
        difference = attended[:prop] - lam * attended[prop:]
        squared = difference * difference
        one = jnp.sum(jnp.where(low, squared, 0.0), axis=1, keepdims=True)
        two = jnp.sum(jnp.where(low, 0.0, squared), axis=1, keepdims=True)
        mean = jnp.where(low, one, two) / HEAD
        norm_all[p, me] = (difference * lax.rsqrt(mean + epsilon) * gain).astype(bf16)
        for to in peers:
            remote(norm_all.at[p, me], norm_all.at[p, me], g_s, g_r.at[p], "kv", to).start()

    def project(p):
        drain(q_recv.at[p], g_r.at[p])
        normed = jnp.concatenate(
            [
                jnp.concatenate([norm_all[p, c * groups + r] for r in range(groups)], axis=0)
                for c in range(cols)
            ],
            axis=1,
        )
        out_part[p] = jnp.dot(normed, wo_buf[...], preferred_element_type=f32).astype(bf16)
        for k in range(1, t):
            remote(out_part.at[p], out_recv.at[p, k - 1], t_s, t_r.at[p], "tp", lax.rem(mine + k, t)).start()

    def finish(p):
        drain(out_recv.at[p], t_r.at[p])
        mixed = out_part[p].astype(f32)
        for k in range(t - 1):
            mixed = mixed + out_recv[p, k].astype(f32)
        for r in range(groups):
            b = r * per + p
            out_ref[b * prop : (b + 1) * prop, :] = mixed[r * prop : (r + 1) * prop].astype(bf16)

    steps = [lambda: (kv_across_x(), kv_send(0))]
    for i in range(len(bits) - 1):
        steps.append(lambda i=i: (kv_take(i), kv_send(i + 1)))
    steps.append(lambda: (kv_take(len(bits) - 1), tree(), kv_up()))
    for p in range(per):
        drain(q_recv.at[p], qa_r.at[p])
        attend(p)
        if p in (0, 2):
            steps.pop(0)()
    while steps:
        steps.pop(0)()
    merged_upto = 0
    weights[3].wait()
    for p in range(merged_upto, per):
        merge(p)
        if p == 1 or p == per - 1 and per < 2:
            kv_spread()
    for p in range(per):
        project(p)
    for p in range(per):
        finish(p)
    kv_end()
    drain(sq_all.at[pl.ds(0, n - 1)], sq_s)
    drain(q_recv, q_s)
    drain(q_recv, qa_s)
    drain(kvx_recv, kx_s)
    drain(st_recv, st_s)
    drain(bv_recv, b_s)
    drain(q_recv, g_s)
    drain(out_recv, t_s)


def place_kernel(
    groups, prop, len_ref, acc_ref, mixed_ref, kv_ref, kbuf_in, vbuf_in, out_hbm, nk_hbm, nv_hbm, kbuf, vbuf,
    k_out, v_out, m_out,
):
    seqs, length, width = kbuf.shape
    cols = width // LANES
    per = seqs // groups
    chunks = kv_ref.shape[0]
    offset = lax.axis_index("kv") * length
    mixed = pltpu.make_async_copy(mixed_ref, out_hbm, m_out)
    mixed.start()
    stores = []
    window = 48
    for b in range(seqs):
        r, begin = b // per, (b % per) * prop
        rel = len_ref[b] + acc_ref[b] - offset
        base = jnp.clip((rel // 16) * 16, 0, length - window)
        at = pl.ds(pl.multiple_of(base, 16), window)
        slot = iota((window, prop), 0) + base - rel
        placing = (slot == iota((window, prop), 1)).astype(bf16)
        slot_col = iota((window, 1), 0) + base - rel
        inside = (slot_col >= 0) & (slot_col < prop)
        for which, buf in enumerate((kbuf, vbuf)):
            fresh = jnp.concatenate(
                [
                    kv_ref[
                        (c * groups + r) % chunks,
                        (c * groups + r) // chunks,
                        begin : begin + prop,
                        which * LANES : (which + 1) * LANES,
                    ]
                    for c in range(cols)
                ],
                axis=1,
            )
            moved = jnp.dot(placing, fresh, preferred_element_type=f32)
            old = buf[b, at, :].astype(f32)
            buf[b, at, :] = jnp.where(inside, moved, old).astype(bf16)
            into, sem = ((nk_hbm, k_out), (nv_hbm, v_out))[which]
            stores.append(pltpu.make_async_copy(buf.at[b], into.at[b], sem.at[b]))
            stores[-1].start()
    for copy in stores:
        copy.wait()
    mixed.wait()


def local(
    n, t, tokens, norm_gain, w_query, w_key, w_value, w_output, cache_keys, cache_values,
    map_lambda, out_gain, parents, lengths, accepted,
):
    rows, depth = tokens.shape
    seqs, length, width = cache_keys.shape
    prop = rows // seqs
    both = 2 * prop
    cols = min(n, width // LANES)
    groups = n // cols
    part = rows // groups
    per = seqs // groups
    out_cols = w_output.shape[1]
    inner_n = math.gcd(n, 1 << (n.bit_length() - 1) // 2)
    outer_n = n // inner_n
    stages = outer_n.bit_length() - 1
    vmem = pl.BlockSpec(memory_space=pltpu.VMEM)
    smem = pl.BlockSpec(memory_space=pltpu.SMEM)
    hbm = pl.BlockSpec(memory_space=pl.ANY)
    dma = pltpu.SemaphoreType.DMA
    V = pltpu.VMEM
    grant = 67043328 - 2 * (2 * cache_keys.size + rows * out_cols + n * part * 2 * LANES) - (1 << 14)
    mixed, gathered, keys, values, held, taken = pl.pallas_call(
        functools.partial(main_kernel, n, t, cols, seqs, prop, depth * n, inner_n),
        name="attend",
        out_shape=(
            V((rows, out_cols), bf16),
            V((n // 2, 2, part, 2 * LANES), bf16),
            V(cache_keys.shape, bf16),
            V(cache_values.shape, bf16),
            V(lengths.shape, jnp.int32),
            V(accepted.shape, jnp.int32),
        ),
        in_specs=[hbm] * 13,
        out_specs=(vmem,) * 6,
        scratch_shapes=[
            V(tokens.shape, bf16),
            V((1, depth), f32),
            V((1, map_lambda.shape[0]), f32),
            V((1, width), f32),
            V(parents.shape, jnp.int32),
            pltpu.SMEM(lengths.shape, jnp.int32),
            pltpu.SMEM(accepted.shape, jnp.int32),
            V((3, depth, width), bf16),
            V(w_output.shape, bf16),
            V((per, n, prop, LANES), bf16),
            V((per, n - 1, prop, LANES), bf16),
            V((per, n, prop, LANES), bf16),
            V((inner_n, outer_n, part, 2 * LANES), bf16),
            V((inner_n - 1, outer_n, part, 2 * LANES), bf16),
            V((outer_n, part, 2 * LANES), bf16),
            V((stages, outer_n // 2, part, 2 * LANES), bf16),
            V((n, 1, LANES), f32),
            V((per, n, 2 * prop, LANES), bf16),
            V((per, n - 1, 2 * prop, LANES), bf16),
            V((per, n, 4, LANES), f32),
            V((per, n - 1, 4, LANES), f32),
            V((per, 2 * prop, LANES), f32),
            V((per, 4, LANES), f32),
            V((per, n, prop, LANES), bf16),
            V((per, groups * prop, out_cols), bf16),
            V((per, t - 1, groups * prop, out_cols), bf16),
            dma((9,)),
            dma((4,)),
            dma((seqs,)),
            dma((seqs,)),
            dma, dma,
            dma, dma((per,)),
            dma, dma((per,)),
            dma, dma,
            dma((stages,)), dma((stages,)),
            dma, dma,
            dma, dma,
            dma, dma((per,)),
            dma, dma((per,)),
            dma, dma((per,)),
            dma, dma((per,)),
        ],
        compiler_params=pltpu.CompilerParams(
            collective_id=0, has_side_effects=True, vmem_limit_bytes=grant
        ),
    )(
        tokens, norm_gain[None], map_lambda[None], out_gain[None], parents, lengths, accepted,
        w_query, w_key, w_value, w_output, cache_keys, cache_values,
    )
    mixed, new_keys, new_values, _, _ = pl.pallas_call(
        functools.partial(place_kernel, groups, prop),
        name="place",
        out_shape=(
            jax.ShapeDtypeStruct(mixed.shape, bf16),
            jax.ShapeDtypeStruct(cache_keys.shape, bf16),
            jax.ShapeDtypeStruct(cache_values.shape, bf16),
            V(cache_keys.shape, bf16),
            V(cache_values.shape, bf16),
        ),
        in_specs=[smem, smem, vmem, vmem, vmem, vmem],
        out_specs=(hbm, hbm, hbm, vmem, vmem),
        input_output_aliases={4: 3, 5: 4},
        scratch_shapes=[dma((seqs,))] * 2 + [dma],
        compiler_params=pltpu.CompilerParams(vmem_limit_bytes=16 << 20),
    )(held, taken, mixed, gathered, keys, values)
    return (mixed, new_keys, new_values)


def solution(mesh):
    placed = (
        P(None, "kv"),
        P("kv"),
        P("kv", "tp"),
        P("kv", "tp"),
        P("kv", "tp"),
        P("tp", "kv"),
        P(None, "kv", "tp"),
        P(None, "kv", "tp"),
        P("tp"),
        P("tp"),
        P(),
        P(),
        P(),
    )
    return jax.shard_map(
        functools.partial(local, mesh.shape["kv"], mesh.shape["tp"]),
        mesh=mesh,
        in_specs=placed,
        out_specs=(P(None, "kv"), P(None, "kv", "tp"), P(None, "kv", "tp")),
        check_vma=False,
    )
```

time: 57.7 us -> 51 us (0.88)
  Pallas kernels: 55.9 us -> 50.2 us
  local copies, waits for them, and re-layouts: 0.65 us -> 0 us
    pallas_call x1, Pallas kernels: 7.53 us -> 4.14 us  [local(): pl.pallas_call(functools.partial(place_kernel, groups, prop), name='place...]
    pallas_call x1, Pallas kernels: 48.3 us -> 46 us  [local(): pl.pallas_call(functools.partial(main_kernel, n, t, cols, seqs, prop, dep...]
    unnamed x3 -> x0, local copies, waits for them, and re-layouts: 0.65 us -> none
where the time goes in v1:
time: 51 us; the launch traced here: 50.8 us
  Pallas kernels  50.2 us (98%)
  between operations  0.64 us (1%)
    pallas_call x1, Pallas kernels, local(): pl.pallas_call(functools.partial(main_kernel, n, t, cols, seqs, prop, dep...  46 us
    pallas_call x1, Pallas kernels, local(): pl.pallas_call(functools.partial(place_kernel, groups, prop), name='place...  4.14 us

profile of v1, /device:TPU:0, one launch (start us, length us, event | category | flops | bytes accessed | tf_op | source)
XLA Modules:
  0.0 50.8 jit_solution(15031807651119617148)
XLA Ops:
  0.6 46.0 %attend.1 = (bf16[96,512]{1,0:T(8,128)(2,1)S(1)}, bf16[4,2,96,256]{3,2,1,0:T(8,128)(2,1)S(1)}, bf16[4,512,1024]{2,1,0:T(8,128)(2,1)S(1)}, bf16[4,512,1024]{2,1,0...) custom-call(bf16[96,512]{1,0:T(8,128)(2,1)} %tok_hbm.1, f32[1,512]{1,0:T(1,128)} %bitcast.4, f32[1,16]{1,0:T(1,128)} %bitcast.5, ...), custom_call_target="tpu_custom_call" | custom-call | tf_op jit(solution)/shard_map/attend/pallas_call | solution.py:488
  46.7 4.1 %place.1 = (bf16[96,512]{1,0:T(8,128)(2,1)}, bf16[4,512,1024]{2,1,0:T(8,128)(2,1)}, bf16[4,512,1024]{2,1,0:T(8,128)(2,1)}, bf16[4,512,1024]{2,1,0:T(8,128)(2,1)S(1)}, bf16[4,512,1024]{2,1,0:T(8,128)(2,1)S(1)}) custom-call(s32[4]{0:T(128)S(1)} %get-tuple-element.12.len_ref, ...), custom_call_target="tpu_custom_call", output_to_operand_aliasing={{3}: (4, {}), {4}: (5, {})} | custom-call | tf_op jit(solution)/shard_map/place/pallas_call | solution.py:551

commit v2 on v1

--- a/solution.py
+++ b/solution.py
@@ -60,9 +60,9 @@
     wq_hbm, wk_hbm, wv_hbm, wo_hbm, keys_hbm, vals_hbm,
     out_ref, kv_ref, kbuf, vbuf, len_out, acc_out,
     tok_ref, gain_ref, lam_ref, out_gain_ref, parent_ref, len_ref, acc_ref,
-    wbuf, wo_buf, q_part, q_recv, q_all, kv_part, kvx_recv, kv_sum, kvz_recv, sq_all,
+    wbuf, wo_buf, q_part, q_recv, q_all, k_cells, v_cells, kx_recv, vx_recv, kz_recv, vz_recv, v1_recv, sq_all,
     bv, bv_recv, st, st_recv, self_v, self_st, norm_all, out_part, out_recv,
-    s_in, w_in, k_in, v_in, sq_s, sq_r, q_s, q_r, qa_s, qa_r, kx_s, kx_r, kz_s, kz_r, up_s, up_r, ag_s, ag_r,
+    s_in, w_in, k_in, v_in, sq_s, sq_r, q_s, q_r, qa_s, qa_r, kx_s, kx_r, vx_s, vx_r, kz_s, kz_r, vz_s, vz_r, up_s, up_r, ag_s, ag_r,
     b_s, b_r, st_s, st_r, g_s, g_r, t_s, t_r,
 ):
     me = lax.axis_index("kv")
@@ -74,10 +74,17 @@
     both = 2 * prop
     _, length, width = kbuf.shape
     scale = QK ** (-0.5)
-    peers = [lax.rem(me + k, n) for k in range(1, n)]
+    others = [lax.rem(me + k, n) for k in range(1, n)]
     outer_n = n // inner_n
     half = outer_n // 2
     x, z = lax.rem(me, inner_n), me // inner_n
+    toward = 1 - 2 * (z // half)
+    peers = []
+    for dz in reversed(range(outer_n)):
+        for dx in reversed(range(inner_n)):
+            if dz or dx:
+                to_z = lax.rem(z + toward * dz + outer_n, outer_n)
+                peers.append(to_z * inner_n + lax.rem(x + dx, inner_n))
     x_peers = [lax.rem(x + k, inner_n) for k in range(1, inner_n)]
     slot = lax.rem(z, half) * inner_n + x
     flat = half * inner_n - 1
@@ -135,22 +142,31 @@
         q_part[p, d] = piece
 
     def place_k(p, d, piece):
-        kv_part[d % inner_n, d // inner_n, p * prop : (p + 1) * prop, :LANES] = piece
+        k_cells[d % inner_n, d // inner_n, p * prop : (p + 1) * prop] = piece
 
     def place_v(p, d, piece):
-        kv_part[d % inner_n, d // inner_n, p * prop : (p + 1) * prop, LANES:] = piece
+        v_cells[d // inner_n, d % inner_n, p * prop : (p + 1) * prop] = piece
 
     products(0, place_q)
     pl.semaphore_wait(barrier, count)
     for to in peers:
         remote(sq_all.at[me], sq_all.at[me], sq_s, sq_r, "kv", to).start()
     for p in range(per):
-        for k, to in enumerate(peers):
-            remote(q_part.at[p, to], q_recv.at[p, k], q_s, q_r.at[p], "kv", to).start()
+        for to in peers:
+            remote(q_part.at[p, to], q_recv.at[p, me], q_s, q_r.at[p], "kv", to).start()
     products(1, place_k)
+    for k, to in enumerate(x_peers):
+        remote(k_cells.at[to], kx_recv.at[k], kx_s, kx_r, "kv", z * inner_n + to).start()
     products(2, place_v)
-    for k, to in enumerate(x_peers):
-        remote(kv_part.at[to], kvx_recv.at[k], kx_s, kx_r, "kv", z * inner_n + to).start()
+    chunks = [z]
+    bits = [1 << i for i in range(outer_n.bit_length() - 1)]
+    live = {}
+    for i in reversed(range(len(bits))):
+        live[i] = chunks
+        chunks = chunks + [flip(c, bits[i]) for c in chunks]
+    near = flip(z, 1) * inner_n + x
+    for i, c in enumerate(live[0]):
+        remote(v_cells.at[flip(c, 1)], vz_recv.at[i], vz_s.at[0], vz_r.at[0], "kv", near).start()
 
     lane = iota((1, LANES), 1)
     low = lane < HEAD
@@ -186,46 +202,59 @@
     mean = jnp.sum(jnp.where(picked, squares, 0.0), axis=1, keepdims=True) / features
     factor = lax.rsqrt(mean + epsilon)
     for p in range(per):
-        drain(q_recv.at[p], q_r.at[p])
+        drain(q_recv.at[p, pl.ds(0, n - 1)], q_r.at[p])
         total = q_part[p, me].astype(f32)
-        for k in range(n - 1):
-            total = total + q_recv[p, k].astype(f32)
+        for d in others:
+            total = total + q_recv[p, d].astype(f32)
         q_all[p, me] = (total * factor[p * prop : (p + 1) * prop]).astype(bf16)
         for to in peers:
             remote(q_all.at[p, me], q_all.at[p, me], qa_s, qa_r.at[p], "kv", to).start()
 
-    def kv_across_x():
-        drain(kvx_recv, kx_r)
+    def add(cells, at, received):
+        total = cells[at].astype(f32)
+        for piece in received:
+            total = total + piece.astype(f32)
+        cells[at] = total.astype(bf16)
+
+    def k_after_x():
+        drain(kx_recv, kx_r)
         for i in range(outer_n):
-            summed = kv_part[x, i].astype(f32)
-            for k in range(inner_n - 1):
-                summed = summed + kvx_recv[k, i].astype(f32)
-            kv_sum[i] = summed.astype(bf16)
-
-    chunks = [z]
-    bits = []
-    bit = 1
-    while bit < outer_n:
-        bits.append(bit)
-        bit *= 2
-    live = {}
-    for s in reversed(range(len(bits))):
-        live[s] = list(chunks)
-        chunks = chunks + [flip(c, bits[s]) for c in chunks]
-
-    def kv_send(s):
-        partner = flip(z, bits[s])
+            add(k_cells, (x, i), [kx_recv[k, i] for k in range(inner_n - 1)])
+
+    def k_send(s):
+        to = flip(z, bits[s]) * inner_n + x
         for i, c in enumerate(live[s]):
-            remote(
-                kv_sum.at[flip(c, bits[s])], kvz_recv.at[s, i], kz_s.at[s], kz_r.at[s], "kv", partner * inner_n + x
-            ).start()
-
-    def kv_take(s):
+            remote(k_cells.at[x, flip(c, bits[s])], kz_recv.at[s, i], kz_s.at[s], kz_r.at[s], "kv", to).start()
+
+    def k_take(s):
         size = len(live[s])
-        drain(kvz_recv.at[s, pl.ds(0, size)], kz_r.at[s])
-        drain(kvz_recv.at[s, pl.ds(0, size)], kz_s.at[s])
+        drain(kz_recv.at[s, pl.ds(0, size)], kz_r.at[s])
         for i, c in enumerate(live[s]):
-            kv_sum[c] = (kv_sum[c].astype(f32) + kvz_recv[s, i].astype(f32)).astype(bf16)
+            add(k_cells, (x, c), [kz_recv[s, i]])
+
+    def v_after_z():
+        drain(vz_recv, vz_r.at[0])
+        for i, c in enumerate(live[0]):
+            for k in range(inner_n):
+                add(v_cells, (c, k), [vz_recv[i, k]])
+        for k, to in enumerate(x_peers):
+            for i, c in enumerate(live[0]):
+                remote(v_cells.at[c, to], vx_recv.at[k, i], vx_s, vx_r, "kv", z * inner_n + to).start()
+
+    def v_after_x():
+        drain(vx_recv, vx_r)
+        for i, c in enumerate(live[0]):
+            add(v_cells, (c, x), [vx_recv[k, i] for k in range(inner_n - 1)])
+
+    def v_send(s):
+        to = flip(z, bits[s]) * inner_n + x
+        for i, c in enumerate(live[s]):
+            remote(v_cells.at[flip(c, bits[s]), x], v1_recv.at[s, i], vz_s.at[s], vz_r.at[s], "kv", to).start()
+
+    def v_take(s):
+        drain(v1_recv.at[s, pl.ds(0, len(live[s]))], vz_r.at[s])
+        for i, c in enumerate(live[s]):
+            add(v_cells, (c, x), [v1_recv[s, i]])
 
     wide_lane = iota((1, 2 * LANES), 1)
 
@@ -269,26 +298,29 @@
         )
         for d in range(n):
             st[p, d] = turned[4 * d : 4 * d + 4]
-        for k, to in enumerate(peers):
-            remote(st.at[p, to], st_recv.at[p, k], st_s, st_r.at[p], "kv", to).start()
-        for k, to in enumerate(peers):
-            remote(bv.at[p, to], bv_recv.at[p, k], b_s, b_r.at[p], "kv", to).start()
+
+    def exchange(p):
+        for to in peers:
+            remote(st.at[p, to], st_recv.at[p, me], st_s, st_r.at[p], "kv", to).start()
+            remote(bv.at[p, to], bv_recv.at[p, me], b_s, b_r.at[p], "kv", to).start()
 
     def tree():
-        own = (kv_sum[z].astype(f32) * factor).astype(bf16)
-        kv_ref[slot, z // half] = own
+        key = (k_cells[x, z].astype(f32) * factor).astype(bf16)
+        value = (v_cells[z, x].astype(f32) * factor).astype(bf16)
+        kv_ref[slot, z // half, :, :LANES] = key
+        kv_ref[slot, z // half, :, LANES:] = value
         query = jnp.concatenate([q_all[p, me] for p in range(per)], axis=0).astype(f32)
         spread = jnp.concatenate(
             [jnp.where(lane // QK == i, query, 0.0) for i in range(4)], axis=0
         ).astype(bf16)
         scores = lax.dot_general(
-            spread, own[:, :LANES], (((1,), (1,)), ((), ())), preferred_element_type=f32
+            spread, key, (((1,), (1,)), ((), ())), preferred_element_type=f32
         )
         scores = jnp.where(lineage, scores * scale, masked_low)
         top = jnp.max(scores, axis=1, keepdims=True)
         weight = jnp.where(lineage, jnp.exp(scores - top), 0.0)
         total = jnp.sum(weight, axis=1, keepdims=True)
-        summed = jnp.dot(weight.astype(bf16), own[:, LANES:], preferred_element_type=f32)
+        summed = jnp.dot(weight.astype(bf16), value, preferred_element_type=f32)
         stat = jnp.zeros((both, LANES), f32)
         for p in range(per):
             cut = [slice(i * part + p * prop, i * part + (p + 1) * prop) for i in range(4)]
@@ -339,9 +371,9 @@
     gain = out_gain_ref[:, pl.ds(pl.multiple_of(col * LANES, LANES), LANES)]
 
     def merge(p):
-        drain(st_recv.at[p], st_r.at[p])
-        drain(bv_recv.at[p], b_r.at[p])
-        stats = [st[p, me]] + [st_recv[p, k] for k in range(n - 1)] + [self_st[p]]
+        drain(st_recv.at[p, pl.ds(0, n - 1)], st_r.at[p])
+        drain(bv_recv.at[p, pl.ds(0, n - 1)], b_r.at[p])
+        stats = [st[p, me]] + [st_recv[p, d] for d in others] + [self_st[p]]
         highest = functools.reduce(jnp.maximum, [a[:2] for a in stats])
         shares = [jnp.exp(a[:2] - highest) for a in stats]
         denominator = functools.reduce(lambda a, b: a + b, [a * b[2:] for a, b in zip(shares, stats)])
@@ -349,7 +381,7 @@
         shares = [a * inverse for a in shares]
         filler = jnp.zeros((LANES - 2 * len(shares), LANES), f32)
         turned = jnp.transpose(jnp.concatenate(shares + [filler], axis=0))
-        values = [bv[p, me]] + [bv_recv[p, k] for k in range(n - 1)] + [self_v[p]]
+        values = [bv[p, me]] + [bv_recv[p, d] for d in others] + [self_v[p]]
         attended = jnp.zeros((both, LANES), f32)
         for i, value in enumerate(values):
             share = jnp.where(low, turned[:both, 2 * i : 2 * i + 1], turned[:both, 2 * i + 1 : 2 * i + 2])
@@ -364,7 +396,7 @@
             remote(norm_all.at[p, me], norm_all.at[p, me], g_s, g_r.at[p], "kv", to).start()
 
     def project(p):
-        drain(q_recv.at[p], g_r.at[p])
+        drain(q_recv.at[p, pl.ds(0, n - 1)], g_r.at[p])
         normed = jnp.concatenate(
             [
                 jnp.concatenate([norm_all[p, c * groups + r] for r in range(groups)], axis=0)
@@ -385,35 +417,46 @@
             b = r * per + p
             out_ref[b * prop : (b + 1) * prop, :] = mixed[r * prop : (r + 1) * prop].astype(bf16)
 
-    steps = [lambda: (kv_across_x(), kv_send(0))]
-    for i in range(len(bits) - 1):
-        steps.append(lambda i=i: (kv_take(i), kv_send(i + 1)))
-    steps.append(lambda: (kv_take(len(bits) - 1), tree(), kv_up()))
+    k_after_x()
+    k_send(0)
+    v_after_z()
+    last = len(bits) - 1
+    steps = [lambda: (v_after_x(), v_send(1))] + [lambda i=i: (k_take(i), k_send(i + 1)) for i in range(last)]
+    steps += [lambda i=i: (v_take(i), v_send(i + 1)) for i in range(1, last)]
     for p in range(per):
-        drain(q_recv.at[p], qa_r.at[p])
+        drain(q_recv.at[p, pl.ds(0, n - 1)], qa_r.at[p])
         attend(p)
-        if p in (0, 2):
+        if p < 2 and steps:
             steps.pop(0)()
-    while steps:
-        steps.pop(0)()
-    merged_upto = 0
+        exchange(p)
+    for step in steps:
+        step()
+    k_take(last)
+    v_take(last)
+    tree()
+    kv_up()
     weights[3].wait()
-    for p in range(merged_upto, per):
+    for p in range(per):
         merge(p)
-        if p == 1 or p == per - 1 and per < 2:
-            kv_spread()
+    kv_spread()
     for p in range(per):
         project(p)
     for p in range(per):
         finish(p)
     kv_end()
     drain(sq_all.at[pl.ds(0, n - 1)], sq_s)
-    drain(q_recv, q_s)
-    drain(q_recv, qa_s)
-    drain(kvx_recv, kx_s)
-    drain(st_recv, st_s)
-    drain(bv_recv, b_s)
-    drain(q_recv, g_s)
+    quiet = q_recv.at[pl.ds(0, per), pl.ds(0, n - 1)]
+    for sem in (q_s, qa_s, g_s):
+        drain(quiet, sem)
+    drain(kx_recv, kx_s)
+    drain(vx_recv, vx_s)
+    drain(vz_recv, vz_s.at[0])
+    for s in range(last + 1):
+        drain(kz_recv.at[s, pl.ds(0, len(live[s]))], kz_s.at[s])
+        if s:
+            drain(v1_recv.at[s, pl.ds(0, len(live[s]))], vz_s.at[s])
+    drain(st_recv.at[pl.ds(0, per), pl.ds(0, n - 1)], st_s)
+    drain(bv_recv.at[pl.ds(0, per), pl.ds(0, n - 1)], b_s)
     drain(out_recv, t_s)
 
 
@@ -509,17 +552,20 @@
             V((3, depth, width), bf16),
             V(w_output.shape, bf16),
             V((per, n, prop, LANES), bf16),
-            V((per, n - 1, prop, LANES), bf16),
             V((per, n, prop, LANES), bf16),
-            V((inner_n, outer_n, part, 2 * LANES), bf16),
-            V((inner_n - 1, outer_n, part, 2 * LANES), bf16),
-            V((outer_n, part, 2 * LANES), bf16),
-            V((stages, outer_n // 2, part, 2 * LANES), bf16),
+            V((per, n, prop, LANES), bf16),
+            V((inner_n, outer_n, part, LANES), bf16),
+            V((outer_n, inner_n, part, LANES), bf16),
+            V((inner_n - 1, outer_n, part, LANES), bf16),
+            V((inner_n - 1, outer_n // 2, part, LANES), bf16),
+            V((stages, outer_n // 2, part, LANES), bf16),
+            V((outer_n // 2, inner_n, part, LANES), bf16),
+            V((stages, outer_n // 2, part, LANES), bf16),
             V((n, 1, LANES), f32),
             V((per, n, 2 * prop, LANES), bf16),
-            V((per, n - 1, 2 * prop, LANES), bf16),
+            V((per, n, 2 * prop, LANES), bf16),
             V((per, n, 4, LANES), f32),
-            V((per, n - 1, 4, LANES), f32),
+            V((per, n, 4, LANES), f32),
             V((per, 2 * prop, LANES), f32),
             V((per, 4, LANES), f32),
             V((per, n, prop, LANES), bf16),
@@ -533,6 +579,8 @@
             dma, dma((per,)),
             dma, dma((per,)),
             dma, dma,
+            dma, dma,
+            dma((stages,)), dma((stages,)),
             dma((stages,)), dma((stages,)),
             dma, dma,
             dma, dma,

time: 51 us -> 46.8 us (0.918)
  Pallas kernels: 50.2 us -> 46 us
    pallas_call x1, Pallas kernels: 46 us -> 41.9 us  [local(): pl.pallas_call(functools.partial(main_kernel, n, t, cols, seqs, prop, dep...]
where the time goes in v2:
time: 46.8 us; the launch traced here: 46.6 us
  Pallas kernels  46 us (98%)
  between operations  0.64 us (1%)
    pallas_call x1, Pallas kernels, local(): pl.pallas_call(functools.partial(main_kernel, n, t, cols, seqs, prop, dep...  41.9 us
    pallas_call x1, Pallas kernels, local(): pl.pallas_call(functools.partial(place_kernel, groups, prop), name='place...  4.14 us

profile of v2, /device:TPU:0, one launch (start us, length us, event | category | flops | bytes accessed | tf_op | source)
XLA Modules:
  0.0 46.6 jit_solution(9716352749628809630)
XLA Ops:
  0.6 41.9 %attend.1 = (bf16[96,512]{1,0:T(8,128)(2,1)S(1)}, bf16[4,2,96,256]{3,2,1,0:T(8,128)(2,1)S(1)}, bf16[4,512,1024]{2,1,0:T(8,128)(2,1)S(1)}, bf16[4,512,1024]{2,1,0...) custom-call(bf16[96,512]{1,0:T(8,128)(2,1)} %tok_hbm.1, f32[1,512]{1,0:T(1,128)} %bitcast.4, f32[1,16]{1,0:T(1,128)} %bitcast.5, ...), custom_call_target="tpu_custom_call" | custom-call | tf_op jit(solution)/shard_map/attend/pallas_call | solution.py:531
  42.5 4.1 %place.1 = (bf16[96,512]{1,0:T(8,128)(2,1)}, bf16[4,512,1024]{2,1,0:T(8,128)(2,1)}, bf16[4,512,1024]{2,1,0:T(8,128)(2,1)}, bf16[4,512,1024]{2,1,0:T(8,128)(2,1)S(1)}, bf16[4,512,1024]{2,1,0:T(8,128)(2,1)S(1)}) custom-call(s32[4]{0:T(128)S(1)} %get-tuple-element.12.len_ref, ...), custom_call_target="tpu_custom_call", output_to_operand_aliasing={{3}: (4, {}), {4}: (5, {})} | custom-call | tf_op jit(solution)/shard_map/place/pallas_call | solution.py:599
